TPU v7x, 32 devices: a whole 2x2x4 slice. The times are simulated.
32 devices in a mesh: sp: 4 (over z), tp: 4 (over y, x), dp: 2 (over core).
Axes of the slice: x: 2, y: 2, z: 4, core: 2. Of those that a mesh axis runs over, the one named last changes fastest.
Arguments:
- latent_in: bfloat16 [3072, 2048], P(('dp', 'sp', 'tp')), parts along dimension 0, may hold values from -6 to 6
- condition: bfloat16 [4096], P(('dp', 'sp')), parts along dimension 0, may hold values from -8 to 8
- context_latent: bfloat16 [1024, 256], P(('dp', 'sp')), parts along dimension 0, may hold values from -6 to 6
- context_rope: bfloat16 [1024, 64], P(('dp', 'sp')), parts along dimension 0, may hold values from -6 to 6
- shift_weight: bfloat16 [2048, 2048], P('sp', 'tp'), may hold values from -0.125 to 0.125
- scale_weight: bfloat16 [2048, 2048], P('sp', 'tp'), may hold values from -0.125 to 0.125
- gate_weight: bfloat16 [2048, 2048], P('sp', 'tp'), may hold values from -0.125 to 0.125
- norm_gain: float32 [2048], replicated, may hold values from 0.1 to 1.9
- down_query: bfloat16 [2048, 512], replicated, may hold values from -0.125 to 0.125
- down_latent: bfloat16 [2048, 256], replicated, may hold values from -0.125 to 0.125
- down_rope: bfloat16 [2048, 64], replicated, may hold values from -0.125 to 0.125
- query_gain: float32 [512], replicated, may hold values from 0.5 to 60
- latent_gain: float32 [256], replicated, may hold values from 0.1 to 1.9
- up_query: bfloat16 [512, 1536], P(None, 'tp'), may hold values from -0.25 to 0.25
- up_key: bfloat16 [256, 1024], P(None, 'tp'), may hold values from -0.375 to 0.375
- up_value: bfloat16 [256, 1024], P(None, 'tp'), may hold values from -0.375 to 0.375
- context_bias: float32 [8], P('tp'), may hold values from 1 to 2.5
- out_weight: bfloat16 [1024, 2048], replicated, may hold values from -3 to 3
Outputs:
- mixed_out: bfloat16 [3072, 2048], P(('dp', 'sp', 'tp')), parts along dimension 0
There are 2 independent parts, one for each index of `dp`. A program takes and returns all parts, laid end to end along the dimension named above; an argument that names none is the same for every part. Nothing has to cross between parts.
All inputs are finite; a program needn't handle non-finite values.
Results may differ from a plain program's by a relative error of at most 0.039.
The roundings to bfloat16 on the way count: a program that leaves them out, or rounds other values in their place, can miss the bound.
Values may be sent and summed in bfloat16 or wider, within the bound.
A program may use at most 128 MiB of HBM per device.

v0:
```python
import jax
import jax.numpy as jnp
from jax import lax
from jax.sharding import PartitionSpec as P

QK_NOPE = 128
QK_ROPE = 64
V_HEAD = 128
GRID_W = 64
epsilon = 1e-06
rope_base = 10000.0
block_limit = 2048


def rms_scaled(values, gain_vec):
    mean_sq = jnp.mean(values * values, axis=-1, keepdims=True)
    return values * lax.rsqrt(mean_sq + epsilon) * gain_vec


def rope_tables(positions, rope_width):
    freq_count = rope_width // 4
    inverse = rope_base ** (-jnp.arange(freq_count, dtype=jnp.float32) / freq_count)
    grid_row = (positions // GRID_W).astype(jnp.float32)
    grid_col = (positions % GRID_W).astype(jnp.float32)
    row_angle = grid_row[:, None] * inverse
    col_angle = grid_col[:, None] * inverse
    angles = jnp.concatenate([row_angle, row_angle, col_angle, col_angle], axis=-1)
    return (jnp.cos(angles), jnp.sin(angles))


def rope_turn(values, cosine_table, sine_table):
    part_one, part_two, part_three, part_four = jnp.split(values, 4, axis=-1)
    turned = jnp.concatenate([-part_two, part_one, -part_four, part_three], axis=-1)
    return values * cosine_table + turned * sine_table


def attend(attn_state, query_nope, query_rope, keys_nope, values_in, keys_rope, bias_col):
    score_scale = (query_nope.shape[-1] + query_rope.shape[-1]) ** (-0.5)
    scores = jnp.einsum("thd,khd->htk", query_nope, keys_nope, preferred_element_type=jnp.float32)
    scores = scores + jnp.einsum(
        "thr,kr->htk", query_rope, keys_rope, preferred_element_type=jnp.float32
    )
    scores = scores * score_scale + bias_col
    run_max, run_total, run_acc = attn_state
    new_max = jnp.maximum(run_max, jnp.max(scores, axis=-1))
    shrink = jnp.exp(run_max - new_max)
    weights = jnp.exp(scores - new_max[:, :, None])
    new_total = run_total * shrink + jnp.sum(weights, axis=-1)
    new_acc = run_acc * shrink[:, :, None] + jnp.einsum(
        "htk,khd->htd", weights.astype(jnp.bfloat16), values_in, preferred_element_type=jnp.float32
    )
    return (new_max, new_total, new_acc)


def over_blocks(attn_state, arrays, handle):
    row_count = arrays[0].shape[0]
    block_rows = 1
    for candidate in range(min(row_count, block_limit), 0, -1):
        if row_count % candidate == 0:
            block_rows = candidate
            break
    block_count = row_count // block_rows
    if block_count == 1:
        return handle(attn_state, arrays)
    stacked = tuple(
        (array_in.reshape((block_count, block_rows) + array_in.shape[1:]) for array_in in arrays)
    )

    def one_turn(inner_state, pieces):
        return (handle(inner_state, pieces), None)

    return lax.scan(one_turn, attn_state, stacked)[0]


def on_device(
    latent_in,
    condition,
    context_latent,
    context_rope,
    shift_weight,
    scale_weight,
    gate_weight,
    norm_gain,
    down_query,
    down_latent,
    down_rope,
    query_gain,
    latent_gain,
    up_query,
    up_key,
    up_value,
    context_bias,
    out_weight,
):
    activated = jax.nn.silu(condition.astype(jnp.float32)).astype(jnp.bfloat16)
    partials = jnp.stack(
        [
            jnp.dot(activated, weight_in, preferred_element_type=jnp.float32)
            for weight_in in (shift_weight, scale_weight, gate_weight)
        ]
    )
    summed = lax.psum(partials, "sp")
    modulation = lax.all_gather(summed, "tp", axis=1, tiled=True)
    shift_vec = modulation[0]
    scale_vec = modulation[1]
    gate_vec = modulation[2]
    residual_in = latent_in.astype(jnp.float32)
    normed = (rms_scaled(residual_in, norm_gain) * (1.0 + scale_vec) + shift_vec).astype(
        jnp.bfloat16
    )
    query_low = rms_scaled(
        jnp.dot(normed, down_query, preferred_element_type=jnp.float32), query_gain
    ).astype(jnp.bfloat16)
    latent_low = rms_scaled(
        jnp.dot(normed, down_latent, preferred_element_type=jnp.float32), latent_gain
    ).astype(jnp.bfloat16)
    local_rows = latent_in.shape[0]
    first_row = (lax.axis_index("sp") * lax.axis_size("tp") + lax.axis_index("tp")) * local_rows
    own_positions = first_row + jnp.arange(local_rows, dtype=jnp.int32)
    own_cosine, own_sine = rope_tables(own_positions, QK_ROPE)
    rope_keys = rope_turn(
        jnp.dot(normed, down_rope, preferred_element_type=jnp.float32), own_cosine, own_sine
    ).astype(jnp.bfloat16)
    query_group, latent_group, rope_group = (
        lax.all_gather(query_low, "tp", axis=0, tiled=True),
        lax.all_gather(latent_low, "tp", axis=0, tiled=True),
        lax.all_gather(rope_keys, "tp", axis=0, tiled=True),
    )
    group_rows = query_group.shape[0]
    group_positions = lax.axis_index("sp") * group_rows + jnp.arange(group_rows, dtype=jnp.int32)
    group_cosine, group_sine = rope_tables(group_positions, QK_ROPE)
    head_count = up_key.shape[1] // QK_NOPE
    queries = jnp.dot(query_group, up_query, preferred_element_type=jnp.float32).reshape(
        group_rows, head_count, QK_NOPE + QK_ROPE
    )
    query_nope = queries[:, :, :QK_NOPE].astype(jnp.bfloat16)
    query_rope = rope_turn(
        queries[:, :, QK_NOPE:], group_cosine[:, None, :], group_sine[:, None, :]
    ).astype(jnp.bfloat16)
    context_all, context_keys_rope = (
        lax.all_gather(context_latent, "sp", axis=0, tiled=True),
        lax.all_gather(context_rope, "sp", axis=0, tiled=True),
    )
    context_count = context_all.shape[0]
    context_nope = (
        jnp.dot(context_all, up_key, preferred_element_type=jnp.float32)
        .astype(jnp.bfloat16)
        .reshape(context_count, head_count, QK_NOPE)
    )
    context_values = (
        jnp.dot(context_all, up_value, preferred_element_type=jnp.float32)
        .astype(jnp.bfloat16)
        .reshape(context_count, head_count, V_HEAD)
    )
    start_state = (
        jnp.full((head_count, group_rows), -jnp.inf, jnp.float32),
        jnp.zeros((head_count, group_rows), jnp.float32),
        jnp.zeros((head_count, group_rows, V_HEAD), jnp.float32),
    )
    bias_col = context_bias[:, None, None]

    def context_step(inner_state, pieces):
        return attend(
            inner_state, query_nope, query_rope, pieces[0], pieces[1], pieces[2], bias_col
        )

    attn_state = over_blocks(
        start_state, (context_nope, context_values, context_keys_rope), context_step
    )
    own_nope = jnp.dot(latent_group, up_key, preferred_element_type=jnp.float32).astype(
        jnp.bfloat16
    )
    own_values = jnp.dot(latent_group, up_value, preferred_element_type=jnp.float32).astype(
        jnp.bfloat16
    )

    def expanded_step(inner_state, pieces):
        piece_rows = pieces[0].shape[0]
        return attend(
            inner_state,
            query_nope,
            query_rope,
            pieces[0].reshape(piece_rows, head_count, QK_NOPE),
            pieces[1].reshape(piece_rows, head_count, V_HEAD),
            pieces[2],
            0.0,
        )

    attn_state = over_blocks(
        attn_state,
        (
            lax.all_gather(own_nope, "sp", axis=0, tiled=True),
            lax.all_gather(own_values, "sp", axis=0, tiled=True),
            lax.all_gather(rope_group, "sp", axis=0, tiled=True),
        ),
        expanded_step,
    )
    attended = (attn_state[2] / attn_state[1][:, :, None]).astype(jnp.bfloat16)
    attended = attended.transpose(1, 0, 2).reshape(group_rows, head_count * V_HEAD)
    token_major = lax.all_to_all(attended, "tp", split_axis=0, concat_axis=1, tiled=True)
    mixed = jnp.dot(token_major, out_weight, preferred_element_type=jnp.float32)
    return (residual_in + gate_vec * mixed).astype(jnp.bfloat16)


def solution(mesh):
    in_specs = (
        P(("dp", "sp", "tp"), None),
        P(("dp", "sp")),
        P(("dp", "sp"), None),
        P(("dp", "sp"), None),
        P("sp", "tp"),
        P("sp", "tp"),
        P("sp", "tp"),
        P(),
        P(),
        P(),
        P(),
        P(),
        P(),
        P(None, "tp"),
        P(None, "tp"),
        P(None, "tp"),
        P("tp"),
        P(),
    )
    out_specs = P(("dp", "sp", "tp"), None)
    return jax.shard_map(
        on_device, mesh=mesh, in_specs=in_specs, out_specs=out_specs, check_vma=False
    )
```

profile of v0, /device:TPU:0, one launch (start us, length us, event | category | flops | bytes accessed | tf_op | source)
XLA Modules:
  0.0 158.6 jit_solution(2897633564219635338)
XLA Ops:
  0.6 0.7 fusion.54
  1.3 1.2 fusion.72
  2.6 1.2 fusion.73
  3.8 1.3 fusion.74
  5.1 13.8 %psum.7 = f32[3,512]{1,0:T(4,128)S(1)} all-reduce(f32[3,512]{1,0:T(4,128)S(1)} %pad_maximum_fusion.2), channel_id=1, replica_groups=mesh['sp'=4,'tp'=4,'dp'=2] {'sp'}, use_global_device_ids=true, to_apply=%region_0.1 | all-reduce | flops 1536 | bytes 12288 | tf_op jit(solution)/shard_map/psum | solution.py:102
  18.9 8.2 %all_gather.27 = f32[3,2048]{1,0:T(4,128)S(1)} all-gather(f32[3,512]{1,0:T(4,128)S(1)} %psum.7), channel_id=1, replica_groups=mesh['sp'=4,'tp'=4,'dp'=2] {'tp'}, dimensions={1}, use_global_device_ids=true | all-gather | bytes 30720 | tf_op jit(solution)/shard_map/all_gather | solution.py:103
  27.1 1.2 fusion.26
  28.4 1.9 %multiply_reduce_fusion.1 = (f32[96]{0:T(128)S(1)}, f32[96,256]{1,0:T(8,128)S(1)}) fusion(bf16[2048,256]{1,0:T(8,128)(2,1)} %param.27, bf16[96,2048]{1,0:T(8,128)(2,1)} %param.18, f32[2048]{0:T(1024)S(1)} %bitcast.119, f32[2048]{0:T(1024)S(1)} %bitcast.122, f32[2048]{0:T(1024)} %param.25, f32[96]{0:T(128)S(1)} %add_rsqrt_fusion.2), kind=kOutput, calls=%fused_computation.50 | convolution fusion | flops 101892000 | bytes 1565440 | tf_op jit(solution)/shard_map/dot_general | solution.py:115
  30.3 8.7 %all_gather.31 = bf16[384,256]{1,0:T(8,128)(2,1)S(1)} all-gather(bf16[96,256]{1,0:T(8,128)(2,1)S(1)} %multiply_convert_fusion.1), channel_id=1, replica_groups=mesh['sp'=4,'tp'=4,'dp'=2] {'tp'}, dimensions={0}, use_global_device_ids=true | all-gather | bytes 245760 | tf_op jit(solution)/shard_map/all_gather | solution.py:126
  39.1 13.8 %all_gather.29 = bf16[512,256]{1,0:T(8,128)(2,1)S(1)} all-gather(bf16[128,256]{1,0:T(8,128)(2,1)S(1)} %copy-done.12), channel_id=1, replica_groups=mesh['sp'=4,'tp'=4,'dp'=2] {'sp'}, dimensions={0}, use_global_device_ids=true | all-gather | bytes 327680 | tf_op jit(solution)/shard_map/all_gather | solution.py:141
  52.9 0.9 convolution_convert_fusion.3
  54.0 1.0 convolution_convert_fusion
  56.0 8.5 %all_gather.28 = bf16[384,512]{1,0:T(8,128)(2,1)S(1)} all-gather(bf16[96,512]{1,0:T(8,128)(2,1)S(1)} %multiply_convert_fusion), channel_id=1, replica_groups=mesh['sp'=4,'tp'=4,'dp'=2] {'tp'}, dimensions={0}, use_global_device_ids=true | all-gather | bytes 491520 | tf_op jit(solution)/shard_map/all_gather | solution.py:125
  65.0 0.7 slice_negate_fusion.1
  66.3 1.3 fusion.62
  67.6 0.6 copy-done.11
  68.9 0.7 broadcast_multiply_fusion.3
  69.6 0.9 fusion.47
  70.5 8.2 %all-gather = bf16[4,96,64]{1,2,0:T(8,128)(2,1)S(1)} all-gather(bf16[1,96,64]{1,2,0:T(8,128)(2,1)S(1)} %fusion.47), channel_id=1, replica_groups=mesh['sp'=4,'tp'=4,'dp'=2] {'tp'}, dimensions={0}, use_global_device_ids=true | all-gather | bytes 61440 | tf_op jit(solution)/shard_map/all_gather | solution.py:127
  78.7 0.7 copy.48
  79.4 1.6 reshape.254
  81.0 14.6 %all_gather.34 = bf16[1536,64]{0,1:T(8,128)(2,1)S(1)} all-gather(bf16[384,64]{0,1:T(8,128)(2,1)} %reshape.254), channel_id=1, replica_groups=mesh['sp'=4,'tp'=4,'dp'=2] {'sp'}, dimensions={0}, use_global_device_ids=true | all-gather | bytes 245760 | tf_op jit(solution)/shard_map/all_gather | solution.py:194
  95.6 16.9 %all_gather.32 = bf16[1536,256]{1,0:T(8,128)(2,1)S(1)} all-gather(bf16[384,256]{1,0:T(8,128)(2,1)} %convolution_convert_fusion.3), channel_id=1, replica_groups=mesh['sp'=4,'tp'=4,'dp'=2] {'sp'}, dimensions={0}, use_global_device_ids=true | all-gather | bytes 983040 | tf_op jit(solution)/shard_map/all_gather | solution.py:192
  112.9 12.2 %all_gather.30 = bf16[512,64]{0,1:T(8,128)(2,1)S(1)} all-gather(bf16[128,64]{0,1:T(8,128)(2,1)S(1)} %copy-done.13), channel_id=1, replica_groups=mesh['sp'=4,'tp'=4,'dp'=2] {'sp'}, dimensions={0}, use_global_device_ids=true | all-gather | bytes 81920 | tf_op jit(solution)/shard_map/all_gather | solution.py:142
  125.4 0.8 fusion.39
  126.3 1.0 fusion.71
  128.3 15.6 %all_gather.35 = bf16[1536,256]{1,0:T(8,128)(2,1)S(1)} all-gather(bf16[384,256]{1,0:T(8,128)(2,1)S(1)} %convolution_convert_fusion.2), channel_id=1, replica_groups=mesh['sp'=4,'tp'=4,'dp'=2] {'sp'}, dimensions={0}, use_global_device_ids=true | all-gather | bytes 983040 | tf_op jit(solution)/shard_map/all_gather | solution.py:193
  143.8 0.8 fusion.1
  144.8 0.7 fusion.19
  145.5 0.9 fusion.23
  146.8 8.1 %all_to_all.19 = bf16[4,96,256]{2,1,0:T(8,128)(2,1)S(1)} all-to-all(bf16[4,96,256]{2,1,0:T(8,128)(2,1)S(1)} %all_to_all.14), channel_id=1, replica_groups=mesh['sp'=4,'tp'=4,'dp'=2] {'tp'}, dimensions={0} | all-to-all | bytes 393216 | tf_op jit(solution)/shard_map/all_to_all | solution.py:200
  154.9 3.8 %fusion.7 = bf16[96,2048]{1,0:T(8,128)(2,1)} fusion(bf16[96,1024]{1,0:T(8,128)(2,1)S(1)} %bitcast.116, bf16[1024,2048]{1,0:T(8,128)(2,1)} %param.35, bf16[96,2048]{1,0:T(8,128)(2,1)S(1)} %copy-done.1, f32[2048]{0:T(1024)S(1)} %bitcast.118), kind=kOutput, calls=%fused_computation.9 | convolution fusion | flops 403439616 | bytes 5185536 | tf_op jit(solution)/shard_map/dot_general | solution.py:201
  (72 shorter events, 5.8 us)
Async XLA Ops:
  0.0 55.3 %copy-start = (bf16[2048,512]{1,0:T(8,128)(2,1)S(1)}, bf16[2048,512]{1,0:T(8,128)(2,1)}, u32[]{:S(2)}) copy-start(bf16[2048,512]{1,0:T(8,128)(2,1)} %param.26) | copy-start | bytes 6291460
  0.0 30.2 %copy-start.19 = (f32[256]{0:T(256)S(1)}, f32[256]{0:T(256)}, u32[]{:S(2)}) copy-start(f32[256]{0:T(256)} %param.30) | copy-start | bytes 3076
  0.0 39.0 %copy-start.12 = (bf16[128,256]{1,0:T(8,128)(2,1)S(1)}, bf16[128,256]{1,0:T(8,128)(2,1)}, u32[]{:S(2)}) copy-start(bf16[128,256]{1,0:T(8,128)(2,1)} %param.20) | copy-start | bytes 196612
  1.3 51.5 %copy-start.3 = (bf16[256,256]{1,0:T(8,128)(2,1)S(1)}, bf16[256,256]{1,0:T(8,128)(2,1)}, u32[]{:S(2)}) copy-start(bf16[256,256]{1,0:T(8,128)(2,1)} %param.32) | copy-start | bytes 393220
  3.8 50.2 %copy-start.4 = (bf16[256,256]{1,0:T(8,128)(2,1)S(1)}, bf16[256,256]{1,0:T(8,128)(2,1)}, u32[]{:S(2)}) copy-start(bf16[256,256]{1,0:T(8,128)(2,1)} %param.33) | copy-start | bytes 393220
  27.1 28.1 %copy-start.14 = (f32[1,2048]{1,0:T(1,128)}, f32[1,2048]{1,0:T(1,128)S(1)}, u32[]{:S(2)}) copy-start(f32[1,2048]{1,0:T(1,128)S(1)} %get-tuple-element.15) | copy-start | bytes 24580
  27.1 27.9 %copy-start.5 = (bf16[256,256]{1,0:T(8,128)(2,1)S(1)}, bf16[256,256]{1,0:T(8,128)(2,1)}, u32[]{:S(2)}) copy-start(bf16[256,256]{1,0:T(8,128)(2,1)} %param.33) | copy-start | bytes 393220
  28.3 26.9 %copy-start.22 = (f32[96]{0:T(128)}, f32[96]{0:T(128)S(1)}, u32[]{:S(2)}) copy-start(f32[96]{0:T(128)S(1)} %add_rsqrt_fusion.2) | copy-start | bytes 1156
  28.3 26.9 %copy-start.1 = (bf16[96,2048]{1,0:T(8,128)(2,1)S(1)}, bf16[96,2048]{1,0:T(8,128)(2,1)}, u32[]{:S(2)}) copy-start(bf16[96,2048]{1,0:T(8,128)(2,1)} %param.18) | copy-start | bytes 1179652
  28.4 26.9 %copy-start.21 = (f32[2048]{0:T(1024)S(1)}, f32[2048]{0:T(1024)}, u32[]{:S(2)}) copy-start(f32[2048]{0:T(1024)} %param.25) | copy-start | bytes 24580
  53.7 2.2 %copy-start.17 = (f32[512]{0:T(512)S(1)}, f32[512]{0:T(512)}, u32[]{:S(2)}) copy-start(f32[512]{0:T(512)} %param.29) | copy-start | bytes 6148
  54.0 10.5 %copy-start.6 = (bf16[512,384]{1,0:T(8,128)(2,1)S(1)}, bf16[512,384]{1,0:T(8,128)(2,1)}, u32[]{:S(2)}) copy-start(bf16[512,384]{1,0:T(8,128)(2,1)} %param.31) | copy-start | bytes 1179652
  67.6 0.6 copy-start.11
  70.5 54.6 %copy-start.15 = (f32[384]{0:T(512)S(1)}, f32[384]{0:T(512)}, u32[]{:S(2)}) copy-start(f32[384]{0:T(512)} %get-tuple-element.33) | copy-start | bytes 4612
  70.5 54.6 %copy-start.16 = (f32[384]{0:T(512)S(1)}, f32[384]{0:T(512)}, u32[]{:S(2)}) copy-start(f32[384]{0:T(512)} %get-tuple-element.34) | copy-start | bytes 4612
  81.0 31.9 %copy-start.13 = (bf16[128,64]{0,1:T(8,128)(2,1)S(1)}, bf16[128,64]{0,1:T(8,128)(2,1)}, u32[]{:S(2)}) copy-start(bf16[128,64]{0,1:T(8,128)(2,1)} %param.21) | copy-start | bytes 49156
  81.0 44.1 %copy-start.18 = (f32[16]{0:T(128)S(1)}, f32[16]{0:T(128)}, u32[]{:S(2)}) copy-start(f32[16]{0:T(128)} %multiply_power_fusion) | copy-start | bytes 196
  81.0 44.4 %copy-start.7 = (f32[384,2,16]{0,2,1:T(8,128)S(1)}, f32[384,2,16]{0,2,1:T(8,128)}, u32[]{:S(2)}) copy-start(f32[384,2,16]{0,2,1:T(8,128)} %get-tuple-element.7) | copy-start | bytes 147460
  81.0 44.4 %copy-start.8 = (f32[384,2,16]{0,2,1:T(8,128)S(1)}, f32[384,2,16]{0,2,1:T(8,128)}, u32[]{:S(2)}) copy-start(f32[384,2,16]{0,2,1:T(8,128)} %get-tuple-element.8) | copy-start | bytes 147460
  81.0 44.4 %copy-start.9 = (f32[384,2,16]{0,2,1:T(8,128)S(1)}, f32[384,2,16]{0,2,1:T(8,128)}, u32[]{:S(2)}) copy-start(f32[384,2,16]{0,2,1:T(8,128)} %get-tuple-element.9) | copy-start | bytes 147460
  81.0 44.4 %copy-start.10 = (f32[384,2,16]{0,2,1:T(8,128)S(1)}, f32[384,2,16]{0,2,1:T(8,128)}, u32[]{:S(2)}) copy-start(f32[384,2,16]{0,2,1:T(8,128)} %get-tuple-element.10) | copy-start | bytes 147460
  126.3 1.0 copy-start.20
  143.8 1.0 copy-start.2
where the time goes:
time: 159 us
  blocking collectives  129 us (81%)
  matrix products  18.4 us (12%)
  other arithmetic  7.9 us (5%)
  local copies, waits for them, and re-layouts  3.43 us (2%)
    all_gather x1, blocking collectives, on_device(): lax.all_gather(own_nope, 'sp', axis=0, tiled=True)  16.9 us
    all_gather x1, blocking collectives, on_device(): lax.all_gather(own_values, 'sp', axis=0, tiled=True)  15.6 us
    all_gather x1, blocking collectives, on_device(): lax.all_gather(rope_group, 'sp', axis=0, tiled=True)  14.6 us
    all_gather x1, blocking collectives, on_device(): lax.all_gather(context_latent, 'sp', axis=0, tiled=True)  13.8 us
    psum x1, blocking collectives, on_device(): summed = lax.psum(partials, 'sp')  13.8 us
    all_gather x1, blocking collectives, on_device(): lax.all_gather(context_rope, 'sp', axis=0, tiled=True)  12.2 us
    all_gather x1, blocking collectives, on_device(): lax.all_gather(latent_low, 'tp', axis=0, tiled=True)  8.7 us
    all_gather x1, blocking collectives, on_device(): lax.all_gather(query_low, 'tp', axis=0, tiled=True)  8.53 us

commit v1 on v0

--- a/solution.py
+++ b/solution.py
@@ -191,7 +191,9 @@
         (
             lax.all_gather(own_nope, "sp", axis=0, tiled=True),
             lax.all_gather(own_values, "sp", axis=0, tiled=True),
-            lax.all_gather(rope_group, "sp", axis=0, tiled=True),
+            jnp.concatenate(
+                lax.all_to_all(jnp.stack([rope_group] * lax.axis_size("sp")), "sp", 0, 0), axis=0
+            ),
         ),
         expanded_step,
     )

time: 159 us -> 153 us (0.962)
  blocking collectives: 129 us -> 115 us
  starting transfers between devices: 0 us -> 3.99 us
  matrix products: 18.4 us -> 21.6 us
  other arithmetic: 7.9 us -> 4.7 us
  local copies, waits for them, and re-layouts: 3.43 us -> 6.42 us
    all_gather x1 -> x0, blocking collectives: 14.6 us -> none  [on_device(): lax.all_gather(rope_group, 'sp', axis=0, tiled=True)]
    all_to_all x0 -> x1, starting transfers between devices: none -> 3.99 us  [on_device(): lax.all_to_all(jnp.stack([rope_group] * lax.axis_size('sp')), 'sp', 0, 0)]
    all_to_all x0 -> x1, local copies, waits for them, and re-layouts: none -> 1.75 us  [on_device(): lax.all_to_all(jnp.stack([rope_group] * lax.axis_size('sp')), 'sp', 0, 0)]
    reshape x0 -> x1, local copies, waits for them, and re-layouts: none -> 1.67 us  [on_device(): jnp.concatenate(lax.all_to_all(jnp.stack([rope_group] * lax.axis_size('sp...]
  transfers between devices with their start and end apart: 0 -> 1, of which waited for: 0 -> 0; matrix products, arithmetic and copies ran while one was open for 0% -> 7% of each run, Pallas kernels for 0% -> 0%
where the time goes in v1:
time: 153 us; the launch traced here: 152 us
  blocking collectives  115 us (75%)
  matrix products  21.6 us (14%)
  local copies, waits for them, and re-layouts  6.42 us (4%)
  other arithmetic  4.7 us (3%)
  starting transfers between devices  3.99 us (3%)
    all_gather x1, blocking collectives, on_device(): lax.all_gather(own_values, 'sp', axis=0, tiled=True)  16.5 us
    all_gather x1, blocking collectives, on_device(): lax.all_gather(own_nope, 'sp', axis=0, tiled=True)  16.1 us
    all_gather x1, blocking collectives, on_device(): lax.all_gather(context_latent, 'sp', axis=0, tiled=True)  14.3 us
    psum x1, blocking collectives, on_device(): summed = lax.psum(partials, 'sp')  13.8 us
    all_gather x1, blocking collectives, on_device(): lax.all_gather(context_rope, 'sp', axis=0, tiled=True)  12.2 us
    all_gather x1, blocking collectives, on_device(): lax.all_gather(query_low, 'tp', axis=0, tiled=True)  9.49 us
    all_gather x1, blocking collectives, on_device(): lax.all_gather(rope_keys, 'tp', axis=0, tiled=True)  8.22 us
    all_gather x1, blocking collectives, on_device(): modulation = lax.all_gather(summed, 'tp', axis=1, tiled=True)  8.2 us
  transfers between devices with their start and end apart: 1, of which 0 were waited for; matrix products, arithmetic and copies ran while one was open for 7% of the time, Pallas kernels for 0%

profile of v1, /device:TPU:0, one launch (start us, length us, event | category | flops | bytes accessed | tf_op | source)
XLA Modules:
  0.0 151.7 jit_solution(1987810659149730762)
XLA Ops:
  0.0 0.8 fusion.52
  0.9 1.2 fusion.70
  2.1 1.2 fusion.71
  3.3 1.2 fusion.72
  4.6 13.8 %psum.7 = f32[3,512]{1,0:T(4,128)S(1)} all-reduce(f32[3,512]{1,0:T(4,128)S(1)} %pad_maximum_fusion.2), channel_id=1, replica_groups=mesh['sp'=4,'tp'=4,'dp'=2] {'sp'}, use_global_device_ids=true, to_apply=%region_0.1 | all-reduce | flops 1536 | bytes 12288 | tf_op jit(solution)/shard_map/psum | solution.py:102
  18.3 8.2 %all_gather.24 = f32[3,2048]{1,0:T(4,128)S(1)} all-gather(f32[3,512]{1,0:T(4,128)S(1)} %psum.7), channel_id=1, replica_groups=mesh['sp'=4,'tp'=4,'dp'=2] {'tp'}, dimensions={1}, use_global_device_ids=true | all-gather | bytes 30720 | tf_op jit(solution)/shard_map/all_gather | solution.py:103
  26.6 1.2 fusion.26
  27.8 1.5 fusion.60
  29.5 8.2 %all-gather = bf16[4,96,64]{1,2,0:T(8,128)(2,1)S(1)} all-gather(bf16[1,96,64]{1,2,0:T(8,128)(2,1)S(1)} %fusion.45), channel_id=1, replica_groups=mesh['sp'=4,'tp'=4,'dp'=2] {'tp'}, dimensions={0}, use_global_device_ids=true | all-gather | bytes 61440 | tf_op jit(solution)/shard_map/all_gather | solution.py:127
  37.9 0.7 stack.23
  38.5 4.0 %all-to-all-start = ((bf16[4,384,64]{1,2,0:T(8,128)(2,1)}), bf16[4,384,64]{1,2,0:T(8,128)(2,1)}, u32[]{:S(2)}, u32[]{:S(2)}) async-start(bf16[4,384,64]{1,2,0:T(8,128)(2,1)} %stack.23), calls=%async_computation | async-start | bytes 393216 | tf_op jit(solution)/shard_map/all_to_all | solution.py:195
  42.6 1.7 %multiply_reduce_fusion.1 = (f32[96]{0:T(128)S(1)}, f32[96,256]{1,0:T(8,128)S(1)}) fusion(bf16[2048,256]{1,0:T(8,128)(2,1)} %param.27, bf16[96,2048]{1,0:T(8,128)(2,1)S(1)} %copy-done.3, f32[2048]{0:T(1024)S(1)} %bitcast.120, f32[2048]{0:T(1024)S(1)} %bitcast.123, f32[2048]{0:T(1024)S(1)} %copy-done.20, f32[96]{0:T(128)S(1)} %add_rsqrt_fusion.2), kind=kOutput, calls=%fused_computation.48 | convolution fusion | flops 101892000 | bytes 1565440 | tf_op jit(solution)/shard_map/dot_general | solution.py:115
  44.4 7.7 %all_gather.28 = bf16[384,256]{1,0:T(8,128)(2,1)S(1)} all-gather(bf16[96,256]{1,0:T(8,128)(2,1)S(1)} %multiply_convert_fusion.1), channel_id=1, replica_groups=mesh['sp'=4,'tp'=4,'dp'=2] {'tp'}, dimensions={0}, use_global_device_ids=true | all-gather | bytes 245760 | tf_op jit(solution)/shard_map/all_gather | solution.py:126
  52.1 14.3 %all_gather.26 = bf16[512,256]{1,0:T(8,128)(2,1)S(1)} all-gather(bf16[128,256]{1,0:T(8,128)(2,1)S(1)} %copy-done.15), channel_id=1, replica_groups=mesh['sp'=4,'tp'=4,'dp'=2] {'sp'}, dimensions={0}, use_global_device_ids=true | all-gather | bytes 327680 | tf_op jit(solution)/shard_map/all_gather | solution.py:141
  66.4 0.9 convolution_convert_fusion.3
  67.3 1.0 convolution_convert_fusion.1
  68.3 1.0 convolution_convert_fusion
  69.2 0.9 convolution_convert_fusion.2
  70.9 9.5 %all_gather.25 = bf16[384,512]{1,0:T(8,128)(2,1)S(1)} all-gather(bf16[96,512]{1,0:T(8,128)(2,1)S(1)} %multiply_convert_fusion), channel_id=1, replica_groups=mesh['sp'=4,'tp'=4,'dp'=2] {'tp'}, dimensions={0}, use_global_device_ids=true | all-gather | bytes 491520 | tf_op jit(solution)/shard_map/all_gather | solution.py:125
  81.5 16.1 %all_gather.29 = bf16[1536,256]{1,0:T(8,128)(2,1)S(1)} all-gather(bf16[384,256]{1,0:T(8,128)(2,1)} %convolution_convert_fusion.3), channel_id=1, replica_groups=mesh['sp'=4,'tp'=4,'dp'=2] {'sp'}, dimensions={0}, use_global_device_ids=true | all-gather | bytes 983040 | tf_op jit(solution)/shard_map/all_gather | solution.py:192
  97.6 1.4 fusion.41
  99.0 12.2 %all_gather.27 = bf16[512,64]{0,1:T(8,128)(2,1)S(1)} all-gather(bf16[128,64]{0,1:T(8,128)(2,1)S(1)} %copy-done.16), channel_id=1, replica_groups=mesh['sp'=4,'tp'=4,'dp'=2] {'sp'}, dimensions={0}, use_global_device_ids=true | all-gather | bytes 81920 | tf_op jit(solution)/shard_map/all_gather | solution.py:142
  112.1 1.2 copy-done.1
  113.7 16.5 %all_gather.31 = bf16[1536,256]{1,0:T(8,128)(2,1)} all-gather(bf16[384,256]{1,0:T(8,128)(2,1)S(1)} %copy-done.8), channel_id=1, replica_groups=mesh['sp'=4,'tp'=4,'dp'=2] {'sp'}, dimensions={0}, use_global_device_ids=true | all-gather | bytes 983040 | tf_op jit(solution)/shard_map/all_gather | solution.py:193
  130.2 1.7 %copy.50 = bf16[4,384,64]{1,0,2:T(4,128)(2,1)} copy(bf16[4,384,64]{1,2,0:T(8,128)(2,1)} %all-to-all-done) | data formatting | bytes 393216 | tf_op jit(solution)/shard_map/all_to_all | solution.py:195
  131.9 1.7 %reshape.268 = bf16[1536,64,1]{0,1,2:T(8,128)(2,1)} reshape(bf16[4,384,64]{1,0,2:T(4,128)(2,1)} %copy.50) | data formatting | bytes 393216 | tf_op jit(solution)/shard_map/reshape | solution.py:194
  133.6 1.8 %fusion.74 = f32[1536,384,2]{0,1,2:T(8,128)S(1)} fusion(bf16[1536,64,1]{0,1,2:T(8,128)(2,1)} %reshape.268, bf16[384,2,64]{0,2,1:T(8,128)(2,1)} %copy-done.6), kind=kOutput, calls=%fused_computation.115 | convolution fusion | flops 150994944 | bytes 5013504 | tf_op jit(solution)/shard_map/thr,kr->htk/dot_general | solution.py:40
  135.4 1.0 fusion.69
  136.5 0.8 fusion.1
  138.6 0.9 fusion.23
  139.8 8.1 %all_to_all.24 = bf16[4,96,256]{2,1,0:T(8,128)(2,1)S(1)} all-to-all(bf16[4,96,256]{2,1,0:T(8,128)(2,1)S(1)} %all_to_all.18), channel_id=1, replica_groups=mesh['sp'=4,'tp'=4,'dp'=2] {'tp'}, dimensions={0} | all-to-all | bytes 393216 | tf_op jit(solution)/shard_map/all_to_all | solution.py:202
  147.9 3.8 %fusion.7 = bf16[96,2048]{1,0:T(8,128)(2,1)} fusion(bf16[96,1024]{1,0:T(8,128)(2,1)S(1)} %bitcast.116, bf16[1024,2048]{1,0:T(8,128)(2,1)} %param.35, bf16[96,2048]{1,0:T(8,128)(2,1)S(1)} %copy-done.4, f32[2048]{0:T(1024)S(1)} %bitcast.118), kind=kOutput, calls=%fused_computation.9 | convolution fusion | flops 403439616 | bytes 5185536 | tf_op jit(solution)/shard_map/dot_general | solution.py:203
  (72 shorter events, 5.2 us)
Async XLA Ops:
  0.0 70.1 %copy-start = (bf16[2048,512]{1,0:T(8,128)(2,1)S(1)}, bf16[2048,512]{1,0:T(8,128)(2,1)}, u32[]{:S(2)}) copy-start(bf16[2048,512]{1,0:T(8,128)(2,1)} %param.26) | copy-start | bytes 6291460
  0.0 42.5 %copy-start.3 = (bf16[96,2048]{1,0:T(8,128)(2,1)S(1)}, bf16[96,2048]{1,0:T(8,128)(2,1)}, u32[]{:S(2)}) copy-start(bf16[96,2048]{1,0:T(8,128)(2,1)} %param.18) | copy-start | bytes 1179652
  0.0 42.5 %copy-start.20 = (f32[2048]{0:T(1024)S(1)}, f32[2048]{0:T(1024)}, u32[]{:S(2)}) copy-start(f32[2048]{0:T(1024)} %param.25) | copy-start | bytes 24580
  26.5 17.7 %copy-start.18 = (f32[256]{0:T(256)S(1)}, f32[256]{0:T(256)}, u32[]{:S(2)}) copy-start(f32[256]{0:T(256)} %param.30) | copy-start | bytes 3076
  27.8 24.3 %copy-start.15 = (bf16[128,256]{1,0:T(8,128)(2,1)S(1)}, bf16[128,256]{1,0:T(8,128)(2,1)}, u32[]{:S(2)}) copy-start(bf16[128,256]{1,0:T(8,128)(2,1)} %param.20) | copy-start | bytes 196612
  27.8 38.6 %copy-start.9 = (bf16[256,256]{1,0:T(8,128)(2,1)S(1)}, bf16[256,256]{1,0:T(8,128)(2,1)}, u32[]{:S(2)}) copy-start(bf16[256,256]{1,0:T(8,128)(2,1)} %param.32) | copy-start | bytes 393220
  37.7 30.6 %copy-start.10 = (bf16[256,256]{1,0:T(8,128)(2,1)S(1)}, bf16[256,256]{1,0:T(8,128)(2,1)}, u32[]{:S(2)}) copy-start(bf16[256,256]{1,0:T(8,128)(2,1)} %param.33) | copy-start | bytes 393220
  38.5 91.6 %all-to-all-start = ((bf16[4,384,64]{1,2,0:T(8,128)(2,1)}), bf16[4,384,64]{1,2,0:T(8,128)(2,1)}, u32[]{:S(2)}, u32[]{:S(2)}) async-start(bf16[4,384,64]{1,2,0:T(8,128)(2,1)} %stack.23), calls=%async_computation | async-start | bytes 393216 | tf_op jit(solution)/shard_map/all_to_all | solution.py:195
  67.3 3.5 %copy-start.17 = (f32[512]{0:T(512)S(1)}, f32[512]{0:T(512)}, u32[]{:S(2)}) copy-start(f32[512]{0:T(512)} %param.29) | copy-start | bytes 6148
  68.3 12.1 %copy-start.11 = (bf16[512,384]{1,0:T(8,128)(2,1)S(1)}, bf16[512,384]{1,0:T(8,128)(2,1)}, u32[]{:S(2)}) copy-start(bf16[512,384]{1,0:T(8,128)(2,1)} %param.31) | copy-start | bytes 1179652
  80.3 18.6 %copy-start.16 = (bf16[128,64]{0,1:T(8,128)(2,1)S(1)}, bf16[128,64]{0,1:T(8,128)(2,1)}, u32[]{:S(2)}) copy-start(bf16[128,64]{0,1:T(8,128)(2,1)} %param.21) | copy-start | bytes 49156
  80.8 30.8 %copy-start.19 = (f32[2]{0:T(128)S(1)}, f32[2]{0:T(128)}, u32[]{:S(2)}) copy-start(f32[2]{0:T(128)} %param.34) | copy-start | bytes 28
  81.5 30.0 %copy-start.12 = (f32[384,2,16]{0,2,1:T(8,128)S(1)}, f32[384,2,16]{0,2,1:T(8,128)}, u32[]{:S(2)}) copy-start(f32[384,2,16]{0,2,1:T(8,128)} %get-tuple-element.8) | copy-start | bytes 147460
  81.5 30.0 %copy-start.13 = (f32[384,2,16]{0,2,1:T(8,128)S(1)}, f32[384,2,16]{0,2,1:T(8,128)}, u32[]{:S(2)}) copy-start(f32[384,2,16]{0,2,1:T(8,128)} %get-tuple-element.9) | copy-start | bytes 147460
  81.5 30.0 %copy-start.14 = (f32[384,2,16]{0,2,1:T(8,128)S(1)}, f32[384,2,16]{0,2,1:T(8,128)}, u32[]{:S(2)}) copy-start(f32[384,2,16]{0,2,1:T(8,128)} %get-tuple-element.10) | copy-start | bytes 147460
  111.6 2.1 %copy-start.6 = (bf16[384,2,64]{0,2,1:T(8,128)(2,1)}, bf16[384,2,64]{0,2,1:T(8,128)(2,1)S(1)}, u32[]{:S(2)}) copy-start(bf16[384,2,64]{0,2,1:T(8,128)(2,1)S(1)} %fusion.38) | copy-start | bytes 294916
  111.6 2.1 %copy-start.8 = (bf16[384,256]{1,0:T(8,128)(2,1)S(1)}, bf16[384,256]{1,0:T(8,128)(2,1)}, u32[]{:S(2)}) copy-start(bf16[384,256]{1,0:T(8,128)(2,1)} %convolution_convert_fusion.2) | copy-start | bytes 589828
  112.1 1.2 copy-start.1
  136.4 1.4 copy-start.2
  136.4 1.4 copy-start.5
  136.4 2.1 %copy-start.7 = (bf16[1536,256]{1,0:T(8,128)(2,1)S(1)}, bf16[1536,256]{1,0:T(8,128)(2,1)}, u32[]{:S(2)}) copy-start(bf16[1536,256]{1,0:T(8,128)(2,1)} %all_gather.31) | copy-start | bytes 2359300
  138.5 9.4 %copy-start.4 = (bf16[96,2048]{1,0:T(8,128)(2,1)S(1)}, bf16[96,2048]{1,0:T(8,128)(2,1)}, u32[]{:S(2)}) copy-start(bf16[96,2048]{1,0:T(8,128)(2,1)} %param.18) | copy-start | bytes 1179652
